TPU v7x, 32 devices: a whole 2x2x4 slice. The times are simulated.
32 devices in a mesh: grp: 2 (over y), sp: 4 (over z), tp: 4 (over x, core).
Axes of the slice: x: 2, y: 2, z: 4, core: 2. Of those that a mesh axis runs over, the one named last changes fastest.
Arguments:
- latents: bfloat16 [2048, 4, 2048], P(('sp', 'tp'), 'grp'), parts along dimension 1, may hold values from -6 to 6
- context: bfloat16 [1024, 4, 2048], P('sp', 'grp'), parts along dimension 1, may hold values from -6 to 6
- condition: float32 [4, 2048], P('grp', 'sp'), parts along dimension 0, may hold values from -6 to 6
- cond_context: float32 [2048], P('sp'), may hold values from -6 to 6
- w_shift: bfloat16 [2048, 2048], P('sp', 'tp'), may hold values from -0.125 to 0.125
- w_scale: bfloat16 [2048, 2048], P('sp', 'tp'), may hold values from -0.125 to 0.125
- w_gate: bfloat16 [2048, 2048], P('sp', 'tp'), may hold values from -0.375 to 0.375
- norm_gain: float32 [2048], replicated, may hold values from 0.1 to 1.9
- w_query: bfloat16 [2048, 1024], P(None, 'tp'), may hold values from -0.375 to 0.375
- w_key: bfloat16 [2048, 512], P(None, 'tp'), may hold values from -0.125 to 0.125
- w_value: bfloat16 [2048, 512], P(None, 'tp'), may hold values from -0.25 to 0.25
- sink_logit: float32 [16], P('tp'), may hold values from 6 to 240
- w_out: bfloat16 [1024, 2048], P('tp'), may hold values from -0.1875 to 0.1875
Outputs:
- refined: bfloat16 [2048, 4, 2048], P(('sp', 'tp'), 'grp'), parts along dimension 1
There are 2 independent parts, one for each index of `grp`. A program takes and returns all parts, laid end to end along the dimension named above; an argument that names none is the same for every part. Nothing has to cross between parts.
All inputs are finite; a program needn't handle non-finite values.
Results may differ from a plain program's by a relative error of at most 0.017.
Values may be sent and summed in bfloat16 or wider, within the bound.
A program may use at most 128 MiB of HBM per device.

v0:
```python
import jax
import jax.numpy as jnp
from jax import lax
from jax.sharding import PartitionSpec as P

HEAD_DIM = 64
WINDOW = 128
GRID_W = 64


EPS = 1e-06
THETA = 10000.0
BIG_NEG = -1e30


def with_halo(cells, sides, width):
    for axis, dim in sides:
        count = lax.axis_size(axis)
        ends = count - 1
        head = lax.slice_in_dim(cells, 0, width, axis=dim)
        tail = lax.slice_in_dim(cells, cells.shape[dim] - width, cells.shape[dim], axis=dim)
        cells = jnp.concatenate(
            [
                lax.ppermute(tail, axis, [(i, (i + 1) % count) for i in range(ends)]),
                cells,
                lax.ppermute(head, axis, [((i + 1) % count, i) for i in range(ends)]),
            ],
            axis=dim,
        )
    return cells


def rotate_pairs(vectors, grid_row, grid_col, head_dim):
    quarter = head_dim // 4
    inverse = THETA ** (-jnp.arange(quarter, dtype=jnp.float32) / quarter)
    angles = jnp.concatenate([grid_row[:, None] * inverse, grid_col[:, None] * inverse], axis=-1)
    shape = (angles.shape[0],) + (1,) * (vectors.ndim - 2) + (head_dim // 2,)
    cosine = jnp.cos(angles).reshape(shape)
    sine = jnp.sin(angles).reshape(shape)
    first_half = vectors[..., : head_dim // 2]
    second_half = vectors[..., head_dim // 2 :]
    return jnp.concatenate(
        [first_half * cosine - second_half * sine, first_half * sine + second_half * cosine],
        axis=-1,
    )


def modulate(tokens_in, gain, shift_rows, scale_rows):
    upcast = tokens_in.astype(jnp.float32)
    normed = upcast * lax.rsqrt(jnp.mean(upcast * upcast, axis=-1, keepdims=True) + EPS)
    return (normed * gain * (1.0 + scale_rows) + shift_rows).astype(jnp.bfloat16)


def on_device(
    latents,
    context,
    condition,
    cond_context,
    w_shift,
    w_scale,
    w_gate,
    norm_gain,
    w_query,
    w_key,
    w_value,
    sink_logit,
    w_out,
):
    samples = latents.shape[1]
    model_width = latents.shape[2]
    n_tp = lax.axis_size("tp")
    n_sp = lax.axis_size("sp")
    local_rows = latents.shape[0]
    tokens = local_rows * n_tp
    local_heads = w_query.shape[1] // HEAD_DIM
    local_kv = w_key.shape[1] // HEAD_DIM
    per_group = local_heads // local_kv
    q_cols = local_heads * HEAD_DIM
    kv_cols = local_kv * HEAD_DIM
    lifted = jax.nn.silu(jnp.concatenate([condition, cond_context[None, :]], axis=0)).astype(
        jnp.bfloat16
    )
    part_shift = jnp.dot(lifted, w_shift, preferred_element_type=jnp.float32)
    part_scale = jnp.dot(lifted, w_scale, preferred_element_type=jnp.float32)
    part_gate = jnp.dot(lifted, w_gate, preferred_element_type=jnp.float32)
    sum_shift, sum_scale, sum_gate = lax.psum((part_shift, part_scale, part_gate), "sp")
    shift_all, scale_all, gate_all = (
        lax.all_gather(sum_shift, "tp", axis=1, tiled=True),
        lax.all_gather(sum_scale, "tp", axis=1, tiled=True),
        lax.all_gather(sum_gate, "tp", axis=1, tiled=True),
    )
    normed = modulate(latents, norm_gain, shift_all[:samples][None], scale_all[:samples][None])
    w_joint = jnp.concatenate([w_query, w_key, w_value], axis=1)
    shard_rows = lax.all_gather(normed, "tp", axis=0, tiled=True)
    row_count = shard_rows.shape[0]
    flat_rows = shard_rows.reshape(row_count * samples, model_width)
    projected = jnp.dot(flat_rows, w_joint, preferred_element_type=jnp.float32).reshape(
        row_count, samples, w_joint.shape[1]
    )
    offset = lax.axis_index("sp") * tokens
    positions = offset + jnp.arange(tokens, dtype=jnp.int32)
    grid_row = (positions // GRID_W).astype(jnp.float32)
    grid_col = (positions % GRID_W).astype(jnp.float32)
    queries = rotate_pairs(
        projected[..., :q_cols].reshape(tokens, samples, local_heads, HEAD_DIM),
        grid_row,
        grid_col,
        HEAD_DIM,
    ).astype(jnp.bfloat16)
    lat_keys = rotate_pairs(
        projected[..., q_cols : q_cols + kv_cols].reshape(tokens, samples, local_kv, HEAD_DIM),
        grid_row,
        grid_col,
        HEAD_DIM,
    ).astype(jnp.bfloat16)
    lat_values = projected[..., q_cols + kv_cols :].astype(jnp.bfloat16)
    paired = jnp.concatenate([lat_keys.reshape(tokens, samples, kv_cols), lat_values], axis=-1)
    extended = with_halo(paired, (("sp", 0),), WINDOW)
    w_pair = jnp.concatenate([w_key, w_value], axis=1)
    ctx_shift = shift_all[samples][None, None]
    ctx_scale = scale_all[samples][None, None]
    ctx_normed = modulate(context, norm_gain, ctx_shift, ctx_scale)
    row_count = context.shape[0]
    flat_ctx = ctx_normed.reshape(row_count * samples, model_width)
    ctx_pairs = lax.all_gather(
        jnp.dot(flat_ctx, w_pair, preferred_element_type=jnp.float32)
        .astype(jnp.bfloat16)
        .reshape(row_count, samples, 2 * kv_cols),
        "sp",
        axis=0,
        tiled=True,
    )
    ctx_len = ctx_pairs.shape[0]
    ctx_keys = ctx_pairs[..., :kv_cols].reshape(ctx_len, samples, local_kv, HEAD_DIM)
    ctx_values = ctx_pairs[..., kv_cols:].reshape(ctx_len, samples, local_kv, HEAD_DIM)
    block_rows = min(tokens, 512)
    n_blocks = tokens // block_rows
    seq_length = tokens * n_sp
    head_sinks = sink_logit.reshape(local_kv, per_group)[None, :, :, None]
    score_scale = HEAD_DIM ** (-0.5)

    def attend_block(block_index):
        first_row = block_index * block_rows
        q_blk = queries.reshape(block_rows, samples, local_kv, per_group, HEAD_DIM)
        k_blk = extended[..., :kv_cols].reshape(
            block_rows + 2 * WINDOW, samples, local_kv, HEAD_DIM
        )
        v_blk = extended[..., kv_cols:].reshape(
            block_rows + 2 * WINDOW, samples, local_kv, HEAD_DIM
        )
        lat_scores = (
            jnp.einsum("qsngd,ksnd->sngqk", q_blk, k_blk, preferred_element_type=jnp.float32)
            * score_scale
        )
        q_pos = offset + first_row + jnp.arange(block_rows, dtype=jnp.int32)
        k_pos = offset + first_row - WINDOW + jnp.arange(block_rows + 2 * WINDOW, dtype=jnp.int32)
        in_window = (
            (jnp.abs(q_pos[:, None] - k_pos[None, :]) <= WINDOW)
            & (k_pos >= 0)[None, :]
            & (k_pos < seq_length)[None, :]
        )
        lat_scores = jnp.where(in_window, lat_scores, BIG_NEG)
        ctx_scores = (
            jnp.einsum("qsngd,ksnd->sngqk", q_blk, ctx_keys, preferred_element_type=jnp.float32)
            * score_scale
        )
        row_max = jnp.maximum(
            jnp.maximum(jnp.max(lat_scores, axis=-1), jnp.max(ctx_scores, axis=-1)), head_sinks
        )
        lat_exp = jnp.exp(lat_scores - row_max[..., None])
        ctx_exp = jnp.exp(ctx_scores - row_max[..., None])
        denominator = (
            jnp.sum(lat_exp, axis=-1) + jnp.sum(ctx_exp, axis=-1) + jnp.exp(head_sinks - row_max)
        )
        lat_weights = (lat_exp / denominator[..., None]).astype(jnp.bfloat16)
        ctx_weights = (ctx_exp / denominator[..., None]).astype(jnp.bfloat16)
        summed = jnp.einsum(
            "sngqk,ksnd->qsngd", lat_weights, v_blk, preferred_element_type=jnp.float32
        )
        summed = summed + jnp.einsum(
            "sngqk,ksnd->qsngd", ctx_weights, ctx_values, preferred_element_type=jnp.float32
        )
        return summed.astype(jnp.bfloat16).reshape(block_rows, samples, q_cols)

    attended = lax.map(attend_block, jnp.arange(n_blocks)).reshape(tokens * samples, q_cols)
    summed_out = lax.psum_scatter(
        jnp.dot(attended, w_out, preferred_element_type=jnp.float32).astype(jnp.bfloat16),
        "tp",
        scatter_dimension=0,
        tiled=True,
    ).astype(jnp.float32)
    mixed = summed_out.reshape(local_rows, samples, model_width)
    refined = latents.astype(jnp.float32) + gate_all[:samples][None] * mixed
    return refined.astype(jnp.bfloat16)


def solution(mesh):
    return jax.shard_map(
        on_device,
        mesh=mesh,
        in_specs=(
            P(("sp", "tp"), "grp", None),
            P("sp", "grp", None),
            P("grp", "sp"),
            P("sp"),
            P("sp", "tp"),
            P("sp", "tp"),
            P("sp", "tp"),
            P(),
            P(None, "tp"),
            P(None, "tp"),
            P(None, "tp"),
            P("tp"),
            P("tp", None),
        ),
        out_specs=P(("sp", "tp"), "grp", None),
        check_vma=False,
    )
```

profile of v0, /device:TPU:13, one launch (start us, length us, event | category | flops | bytes accessed | tf_op | source)
XLA Modules:
  0.0 236.1 jit_solution(7936242793611745387)
XLA Ops:
  6.5 1.4 fusion.49
  7.9 1.3 fusion.51
  9.2 1.3 fusion.53
  10.5 12.1 %all-reduce = (f32[3,512]{1,0:T(4,128)S(1)}, f32[3,512]{1,0:T(4,128)S(1)}, f32[3,512]{1,0:T(4,128)S(1)}) all-reduce(f32[3,512]{1,0:T(4,128)S(1)} %fusion.49, f32[3,512]{1,0:T(4,128)S(1)} %fusion.51, f32[3,512]{1,0:T(4,128)S(1)} %fusion.53), channel_id=1, replica_groups=mesh['grp'=2,'sp'=4,'tp'=4] {'sp'}, use_global_device_ids=true, to_apply=%region_3.4 | all-reduce | flops 4608 | bytes 36864 | tf_op jit(solution)/shard_map/psum | solution.py:86
  22.5 9.2 %all_gather.17 = f32[3,2048]{1,0:T(4,128)S(1)} all-gather(f32[3,512]{1,0:T(4,128)S(1)} %get-tuple-element.19), channel_id=1, replica_groups=mesh['grp'=2,'sp'=4,'tp'=4] {'tp'}, dimensions={1}, use_global_device_ids=true | all-gather | bytes 30720 | tf_op jit(solution)/shard_map/all_gather | solution.py:88
  31.7 5.2 %all_gather.16 = f32[3,2048]{1,0:T(4,128)S(1)} all-gather(f32[3,512]{1,0:T(4,128)S(1)} %get-tuple-element.20), channel_id=1, replica_groups=mesh['grp'=2,'sp'=4,'tp'=4] {'tp'}, dimensions={1}, use_global_device_ids=true | all-gather | bytes 30720 | tf_op jit(solution)/shard_map/all_gather | solution.py:89
  36.9 3.8 %fusion.6 = f32[256,2]{1,0:T(8,128)S(1)} fusion(bf16[256,2,2048]{2,1,0:T(2,128)(2,1)} %param.14), kind=kLoop, calls=%fused_computation.14 | loop fusion | flops 3145216 | bytes 2099200 | tf_op jit(solution)/shard_map/reduce_sum | solution.py:50
  40.8 4.5 %fusion.10 = bf16[256,2,2048]{2,1,0:T(2,128)(2,1)} fusion(bf16[256,2,2048]{2,1,0:T(2,128)(2,1)S(1)} %copy-done.3, f32[2048]{0:T(1024)S(1)} %bitcast.83, f32[2048]{0:T(1024)S(1)} %bitcast.84, f32[2048]{0:T(1024)S(1)} %copy-done.6, f32[256,2]{1,0:T(8,128)S(1)} %add_rsqrt_fusion), kind=kLoop, calls=%fused_computation.18 | loop fusion | flops 6291456 | bytes 4220928 | tf_op jit(solution)/shard_map/convert_element_type | solution.py:51
  45.3 4.2 %reshape.218 = bf16[512,2048]{1,0:T(8,128)(2,1)} reshape(bf16[256,2,2048]{2,1,0:T(2,128)(2,1)} %fusion.10) | data formatting | bytes 4194304 | tf_op jit(solution)/shard_map/reshape | solution.py:124
  49.6 2.4 %convolution_convert_fusion.1 = bf16[512,256]{1,0:T(8,128)(2,1)S(1)} fusion(bf16[512,2048]{1,0:T(8,128)(2,1)} %reshape.218, bf16[2048,128]{1,0:T(8,128)(2,1)S(1)} %copy-done.4, bf16[2048,128]{1,0:T(8,128)(2,1)} %param.22), kind=kOutput, calls=%fused_computation.42 | convolution fusion | flops 539099136 | bytes 3407872 | tf_op jit(solution)/shard_map/dot_general | solution.py:126
  52.0 0.8 reshape.219
  52.8 0.0 all-gather.5.cloned.1.call-update
  52.8 0.0 all-gather.3.cloned.1.call-start
  52.9 0.0 copy-start.8
  52.9 0.4 fusion.11
  53.3 1.6 fusion.15
  54.9 0.0 all-gather.3.cloned.1.call-update
  54.9 0.0 reduce-scatter.2.cloned.1.call-start
  54.9 1.0 copy.60
  56.0 2.0 copy.59
  58.0 2.3 copy.58
  60.3 0.1 max.33
  60.4 0.1 broadcast_multiply_fusion.1
  60.5 0.2 fusion.33
  60.7 0.8 fusion.23
  61.5 19.8 %all-gather.5.cloned.1.call-done = bf16[1024,2,256]{2,1,0:T(2,128)(2,1)} async-done(((bf16[256,2,256]{2,1,0:T(2,128)(2,1)}), bf16[1024,2,256]{2,1,0:T(2,128)(2,1)}) %all-gather.5.cloned.1.call-update) | async-done | bytes 1048592 | tf_op jit(solution)/shard_map/all_gather | solution.py:125
  81.3 2.7 %fusion.55 = (bf16[1024,2,128]{2,1,0:T(2,128)(2,1)}, bf16[1024,2,128]{2,1,0:T(2,128)(2,1)S(1)}) fusion(bf16[1024,2,256]{2,1,0:T(2,128)(2,1)} %all-gather.5.cloned.1.call-done), kind=kLoop, calls=%fused_computation.98 | loop fusion | bytes 2097152 | tf_op jit(solution)/shard_map/slice | solution.py:134
  84.1 1.1 copy.65
  85.2 1.3 copy.63
  86.5 31.5 %all-gather.3.cloned.1.call-done = bf16[512,2,2048]{2,0,1:T(8,128)(2,1)} async-done(((bf16[128,2,2048]{2,0,1:T(8,128)(2,1)}), bf16[512,2,2048]{2,0,1:T(8,128)(2,1)}) %all-gather.3.cloned.1.call-update) | async-done | bytes 4194320 | tf_op jit(solution)/shard_map/all_gather | solution.py:94
  118.0 5.2 %fusion.17 = f32[512,2,512]{0,2,1:T(8,128)S(1)} fusion(bf16[512,2,2048]{2,0,1:T(8,128)(2,1)} %all-gather.3.cloned.1.call-done, bf16[2048,128]{0,1:T(8,128)(2,1)} %copy.60, bf16[2048,128]{0,1:T(8,128)(2,1)} %copy.59, bf16[2048,256]{0,1:T(8,128)(2,1)} %copy.58), kind=kOutput, calls=%fused_computation.30 | convolution fusion | flops 2153775104 | bytes 8388608 | tf_op jit(solution)/shard_map/dot_general | solution.py:97
  123.2 0.1 slice.84
  123.3 0.2 subtract_convert_fusion
  123.5 0.1 subtract_convert_fusion.1
  123.7 2.2 collective-permute-start.1
  125.8 3.3 %collective-permute-start = (bf16[128,2,256]{0,2,1:T(8,128)(2,1)S(1)}, bf16[128,2,256]{0,2,1:T(8,128)(2,1)S(1)}, u32[]{:S(2)}, u32[]{:S(2)}) collective-permute-start(bf16[128,2,256]{0,2,1:T(8,128)(2,1)S(1)} %get-tuple-element.40), channel_id=1, source_target_pairs={{0,4},{4,8},{8,12},{1,5},{5,9},{9,13},{2,6},{6,10},{10,14},{3,7},{... | collective-permute-start | bytes 393224 | tf_op jit(solution)/shard_map/ppermute | solution.py:24
  129.1 8.1 %bitcast_reduce_fusion = (f32[2,2,2,512]{3,2,1,0:T(2,128)S(1)}, f32[2,2,1024,512,2]{3,2,4,1,0:T(8,128)}) fusion(bf16[1024,2,2,64,1]{0,3,4,2,1:T(8,128)(2,1)S(1)} %bitcast.74, bf16[512,2,2,2,32]{0,4,3,2,1:T(8,128)(2,1)S(1)} %bitcast.78, bf16[512,2,2,2,32]{0,4,3,2,1:T(8,128)(2,1)S(1)} %bitcast.76), kind=kOutput, calls=%fused_computation.1 | convolution fusion | flops 546304000 | bytes 17842176 | tf_op jit(solution)/shard_map/while/body/eval_jaxpr/qsngd,ksnd->sngqk/dot_general | solution.py:164
  137.3 0.0 collective-permute-done.1
  137.3 0.0 collective-permute-done
  137.3 0.1 pad_maximum_fusion
  137.4 0.8 fusion.56
  138.2 2.1 fusion.3
  140.3 0.0 copy-start.1
  140.3 0.0 copy-done.7
  140.3 0.1 maximum_maximum_fusion
  140.4 2.6 %fusion.2 = f32[2,2,2,512]{3,2,1,0:T(2,128)S(1)} fusion(f32[2,2,768,512,2]{3,2,4,1,0:T(8,128)S(1)} %get-tuple-element.47, f32[2,2,2,512]{3,2,1,0:T(2,128)S(1)} %maximum_maximum_fusion, pred[512,768]{0,1:T(8,128)(4,1)S(1)} %fusion.23), kind=kLoop, calls=%fused_computation.8 | loop fusion | flops 12578816 | bytes 13008896 | tf_op jit(solution)/shard_map/while/body/eval_jaxpr/reduce_sum | solution.py:173
  143.0 1.8 copy-done.1
  144.9 9.3 %fusion.1 = f32[2,2,2,512]{3,2,1,0:T(2,128)} fusion(f32[2,2,1024,512,2]{3,2,4,1,0:T(8,128)} %get-tuple-element.49, f32[2,2,2,512]{3,2,1,0:T(2,128)S(1)} %maximum_maximum_fusion), kind=kLoop, calls=%fused_computation.4 | loop fusion | flops 12578816 | bytes 16809984 | tf_op jit(solution)/shard_map/while/body/eval_jaxpr/reduce_sum | solution.py:173
  154.2 0.8 exponential_add_fusion
  155.0 0.0 slice-start.1
  155.0 0.0 slice-start.2
  155.0 0.0 copy-start.5
  155.0 8.0 %fusion.4 = f32[2,2,64,2,512]{4,2,3,1,0:T(8,128)S(1)} fusion(bf16[1024,2,2,64,1]{0,3,4,2,1:T(8,128)(2,1)} %bitcast.80, f32[2,2,1024,512,2]{3,2,4,1,0:T(8,128)} %get-tuple-element.49, f32[2,2,2,512]{3,2,1,0:T(2,128)S(1)} %exponential_add_fusion, f32[2,2,2,512]{3,2,1,0:T(2,128)S(1)} %maximum_maximum_fusion), kind=kOutput, calls=%fused_computation.10 | convolution fusion | flops 553648128 | bytes 18382848 | tf_op jit(solution)/shard_map/while/body/eval_jaxpr/sngqk,ksnd->qsngd/dot_general | solution.py:180
  163.1 0.4 slice-done.2
  163.5 4.3 %fusion.26 = bf16[512,2,2,2,64]{0,4,3,2,1:T(8,128)(2,1)} fusion(f32[2,2,64,2,512]{4,2,3,1,0:T(8,128)S(1)} %fusion.4, bf16[768,2,2,64,1]{0,3,4,2,1:T(8,128)(2,1)S(1)} %bitcast.81, f32[2,2,768,512,2]{3,2,4,1,0:T(8,128)S(1)} %bitcast.70, f32[2,2,2,512]{3,2,1,0:T(2,128)S(1)} %exponential_add_fusion, f32[2,2,2,512]{3,2,1,0:T(2,128)S(1)} %maximum_maximum_fusion, ...), kind=kOutput, calls=%fused_computation.41 | convolution fusion | flops 418906112 | bytes 14974976 | tf_op jit(solution)/shard_map/while/body/eval_jaxpr/sngqk,ksnd->qsngd/dot_general | solution.py:177
  167.8 3.6 %copy.67 = bf16[512,2,2,2,64]{4,3,2,1,0:T(2,128)(2,1)} copy(bf16[512,2,2,2,64]{0,4,3,2,1:T(8,128)(2,1)} %fusion.26) | data formatting | bytes 1048576 | tf_op jit(solution)/shard_map/while/body/eval_jaxpr/convert_element_type | solution.py:183
  171.4 2.8 %reshape.222 = bf16[1024,256]{1,0:T(8,128)(2,1)S(1)} reshape(bf16[512,2,2,2,64]{4,3,2,1,0:T(2,128)(2,1)} %copy.67) | data formatting | bytes 1048576 | tf_op jit(solution)/shard_map/reshape | solution.py:185
  174.1 3.2 %convolution_convert_fusion = bf16[1024,2048]{1,0:T(8,128)(2,1)} fusion(bf16[1024,256]{1,0:T(8,128)(2,1)S(1)} %reshape.222, bf16[256,2048]{1,0:T(8,128)(2,1)S(1)} %copy-done), kind=kOutput, calls=%fused_computation.19 | convolution fusion | flops 1075838976 | bytes 5767168 | tf_op jit(solution)/shard_map/dot_general | solution.py:187
  177.3 0.0 reduce-scatter.2.cloned.1.call-update
  177.4 5.9 %all_gather.15 = f32[3,2048]{1,0:T(4,128)S(1)} all-gather(f32[3,512]{1,0:T(4,128)S(1)} %get-tuple-element.21), channel_id=1, replica_groups=mesh['grp'=2,'sp'=4,'tp'=4] {'tp'}, dimensions={1}, use_global_device_ids=true | all-gather | bytes 30720 | tf_op jit(solution)/shard_map/all_gather | solution.py:90
  183.2 37.9 %reduce-scatter.2.cloned.1.call-done = bf16[256,2048]{1,0:T(8,128)(2,1)} async-done(((bf16[1024,2048]{1,0:T(8,128)(2,1)}), bf16[256,2048]{1,0:T(8,128)(2,1)}) %reduce-scatter.2.cloned.1.call-update) | async-done | bytes 1048592 | tf_op jit(solution)/shard_map/reduce_scatter | solution.py:186
  221.2 3.4 %reshape.226 = f32[128,2,2048]{2,1,0:T(2,128)} reshape(bf16[256,2048]{1,0:T(8,128)(2,1)} %reduce-scatter.2.cloned.1.call-done) | data formatting | bytes 3145728 | tf_op jit(solution)/shard_map/reshape | solution.py:192
  224.5 3.0 %fusion.16 = bf16[128,2,2048]{2,0,1:T(8,128)(2,1)S(1)} fusion(f32[128,2,2048]{2,1,0:T(2,128)} %reshape.226, f32[2,2048]{1,0:T(2,128)S(1)} %slice.75, bf16[128,2,2048]{2,1,0:T(2,128)(2,1)S(1)} %copy-done.2), kind=kLoop, calls=%fused_computation.28 | loop fusion | flops 2097152 | bytes 4210688 | tf_op jit(solution)/shard_map/convert_element_type | solution.py:194
  227.5 2.0 copy.69
  (34 shorter events, 0.3 us)
Async XLA Ops:
  6.5 167.6 %copy-start = (bf16[256,2048]{1,0:T(8,128)(2,1)S(1)}, bf16[256,2048]{1,0:T(8,128)(2,1)}, u32[]{:S(2)}) copy-start(bf16[256,2048]{1,0:T(8,128)(2,1)} %param.25) | copy-start | bytes 3145732
  6.5 34.3 %copy-start.3 = (bf16[256,2,2048]{2,1,0:T(2,128)(2,1)S(1)}, bf16[256,2,2048]{2,1,0:T(2,128)(2,1)}, u32[]{:S(2)}) copy-start(bf16[256,2,2048]{2,1,0:T(2,128)(2,1)} %param.14) | copy-start | bytes 6291460
  6.5 34.3 %copy-start.6 = (f32[2048]{0:T(1024)S(1)}, f32[2048]{0:T(1024)}, u32[]{:S(2)}) copy-start(f32[2048]{0:T(1024)} %param.20) | copy-start | bytes 24580
  6.5 74.8 %all-gather.5.cloned.1.call-start = ((), (), s32[]{:S(2)}) async-start(), calls=%async_computation.2 | async-start | bytes 1310720 | tf_op jit(solution)/shard_map/all_gather | solution.py:125
  45.3 4.2 %copy-start.4 = (bf16[2048,128]{1,0:T(8,128)(2,1)S(1)}, bf16[2048,128]{1,0:T(8,128)(2,1)}, u32[]{:S(2)}) copy-start(bf16[2048,128]{1,0:T(8,128)(2,1)} %param.23) | copy-start | bytes 1572868
  45.3 7.5 %copy-start.2 = (bf16[128,2,2048]{2,1,0:T(2,128)(2,1)S(1)}, bf16[128,2,2048]{2,1,0:T(2,128)(2,1)}, u32[]{:S(2)}) copy-start(bf16[128,2,2048]{2,1,0:T(2,128)(2,1)} %param.13) | copy-start | bytes 3145732
  52.8 65.2 %all-gather.3.cloned.1.call-start = ((), (), s32[]{:S(2)}) async-start(), calls=%async_computation.1 | async-start | bytes 5242880 | tf_op jit(solution)/shard_map/all_gather | solution.py:94
  52.9 7.4 %copy-start.8 = (f32[4]{0:T(128)S(1)}, f32[4]{0:T(128)}, u32[]{:S(2)}) copy-start(f32[4]{0:T(128)} %param.24) | copy-start | bytes 52
  54.9 166.3 %reduce-scatter.2.cloned.1.call-start = ((), (), s32[]{:S(2)}) async-start(), calls=%async_computation.3 | async-start | bytes 5242880 | tf_op jit(solution)/shard_map/reduce_scatter | solution.py:186
  60.4 80.0 %copy-start.7 = (f32[2,2]{1,0:T(2,128)}, f32[2,2]{1,0:T(2,128)S(1)}, u32[]{:S(2)}) copy-start(f32[2,2]{1,0:T(2,128)S(1)} %max.33) | copy-start | bytes 52
  123.7 13.6 %collective-permute-start.1 = (bf16[128,2,256]{0,2,1:T(8,128)(2,1)S(1)}, bf16[128,2,256]{0,2,1:T(8,128)(2,1)S(1)}, u32[]{:S(2)}, u32[]{:S(2)}) collective-permute-start(bf16[128,2,256]{0,2,1:T(8,128)(2,1)S(1)} %get-tuple-element.41), channel_id=1, source_target_pairs={{4,0},{8,4},{12,8},{5,1},{9,5},{13,9},{6,2},{10,6},{14,10},{7,3},{... | collective-permute-start | bytes 393224 | tf_op jit(solution)/shard_map/ppermute | solution.py:26
  125.8 11.4 %collective-permute-start = (bf16[128,2,256]{0,2,1:T(8,128)(2,1)S(1)}, bf16[128,2,256]{0,2,1:T(8,128)(2,1)S(1)}, u32[]{:S(2)}, u32[]{:S(2)}) collective-permute-start(bf16[128,2,256]{0,2,1:T(8,128)(2,1)S(1)} %get-tuple-element.40), channel_id=1, source_target_pairs={{0,4},{4,8},{8,12},{1,5},{5,9},{9,13},{2,6},{6,10},{10,14},{3,7},{... | collective-permute-start | bytes 393224 | tf_op jit(solution)/shard_map/ppermute | solution.py:24
  140.3 4.5 %copy-start.1 = (f32[2,2,768,512,2]{3,2,4,1,0:T(8,128)}, f32[2,2,768,512,2]{3,2,4,1,0:T(8,128)S(1)}, u32[]{:S(2)}) copy-start(f32[2,2,768,512,2]{3,2,4,1,0:T(8,128)S(1)} %get-tuple-element.47) | copy-start | bytes 37748740
  144.9 18.2 %slice-start = ((s8[12582912]{0:T(1024)(128)(4,1)}), s8[4194304]{0:T(1024)(128)(4,1)S(1)}, s32[]{:S(2)}) async-start(s8[12582912]{0:T(1024)(128)(4,1)} %bitcast.69), calls=%async_computation.4 | async-start | bytes 8388608
  155.0 8.1 %slice-start.1 = ((s8[12582912]{0:T(1024)(128)(4,1)}), s8[4194304]{0:T(1024)(128)(4,1)S(1)}, s32[]{:S(2)}) async-start(s8[12582912]{0:T(1024)(128)(4,1)} %bitcast.69), calls=%async_computation.5 | async-start | bytes 8388608
  155.0 8.5 %slice-start.2 = ((s8[12582912]{0:T(1024)(128)(4,1)}), s8[4194304]{0:T(1024)(128)(4,1)S(1)}, s32[]{:S(2)}) async-start(s8[12582912]{0:T(1024)(128)(4,1)} %bitcast.69), calls=%async_computation.6 | async-start | bytes 8388608
  155.0 8.5 %copy-start.5 = (bf16[768,2,128]{0,2,1:T(8,128)(2,1)S(1)}, bf16[768,2,128]{0,2,1:T(8,128)(2,1)}, u32[]{:S(2)}) copy-start(bf16[768,2,128]{0,2,1:T(8,128)(2,1)} %get-tuple-element.36) | copy-start | bytes 1179652
Sparse Core Ops, SparseCore 0:
  52.9 28.3 all-gather.4
  82.9 35.0 all-gather.2
  177.5 43.6 reduce-scatter.1
where the time goes:
time: 239 us; the launch traced here: 236 us
  waiting for transfers between devices  89.3 us (37%)
  matrix products  37.3 us (16%)
  blocking collectives  32.3 us (14%)
  local copies, waits for them, and re-layouts  30.5 us (13%)
  other arithmetic  27.7 us (12%)
  between operations  13.4 us (6%)
  starting transfers between devices  5.55 us (2%)
    reduce_scatter x1, waiting for transfers between devices, on_device(): lax.psum_scatter(jnp.dot(attended, w_out, preferred_element_type=jnp.floa...  37.9 us
    all_gather x1, waiting for transfers between devices, on_device(): shard_rows = lax.all_gather(normed, 'tp', axis=0, tiled=True)  31.5 us
    all_gather x1, waiting for transfers between devices, on_device(): lax.all_gather(jnp.dot(flat_ctx, w_pair, preferred_element_type=jnp.float...  19.8 us
    psum x1, blocking collectives, on_device(): lax.psum((part_shift, part_scale, part_gate), 'sp')  12.1 us
    reduce_sum x1, other arithmetic, attend_block(): jnp.sum(ctx_exp, axis=-1)  9.31 us
    all_gather x1, blocking collectives, on_device(): lax.all_gather(sum_shift, 'tp', axis=1, tiled=True)  9.18 us
    dot_general x1, matrix products, attend_block(): jnp.einsum('qsngd,ksnd->sngqk', q_blk, ctx_keys, preferred_element_type=j...  8.13 us
    dot_general x1, matrix products, attend_block(): jnp.einsum('sngqk,ksnd->qsngd', ctx_weights, ctx_values, preferred_elemen...  8.03 us
  transfers between devices with their start and end apart: 5, of which 3 were waited for; matrix products, arithmetic and copies ran while one was open for 9% of the time, Pallas kernels for 0%

commit v1 on v0

v1 whole, which is shorter than its diff:
```python
import functools

import jax
import jax.numpy as jnp
from jax import lax
from jax.experimental import pallas as pl
from jax.experimental.pallas import tpu as pltpu
from jax.sharding import PartitionSpec as P

HEAD_DIM = 64
WINDOW = 128
GRID_W = 64
EPS = 1e-06
THETA = 10000.0
BIG_NEG = -1e30
VMEM_LIMIT = 60 * 1024 * 1024
F32 = jnp.float32
BF16 = jnp.bfloat16
ANY = pl.BlockSpec(memory_space=pl.ANY)
VMEM = pl.BlockSpec(memory_space=pltpu.VMEM)


def enter(peers):
    barrier = pltpu.get_barrier_semaphore()
    for peer in peers:
        pl.semaphore_signal(
            barrier, inc=1, device_id=peer, device_id_type=pl.DeviceIdType.MESH
        )
    pl.semaphore_wait(barrier, len(peers))


def remote(src, dst, send, recv, peer):
    return pltpu.make_async_remote_copy(
        src_ref=src,
        dst_ref=dst,
        send_sem=send,
        recv_sem=recv,
        device_id=peer,
        device_id_type=pl.DeviceIdType.MESH,
    )


def front_kernel(
    n_tp,
    n_sp,
    samples,
    q_cols,
    kv_cols,
    lifted,
    gain,
    cos_t,
    sin_t,
    lat_hbm,
    ctx_hbm,
    ws_hbm,
    wc_hbm,
    wg_hbm,
    *rest,
):
    n_proj = len(rest) - 27
    proj_hbm = rest[:n_proj]
    front_body(
        n_tp, n_sp, samples, q_cols, kv_cols, lifted, gain, cos_t, sin_t,
        lat_hbm, ctx_hbm, ws_hbm, wc_hbm, wg_hbm, proj_hbm, *rest[n_proj:],
    )


def front_body(
    n_tp,
    n_sp,
    samples,
    q_cols,
    kv_cols,
    lifted,
    gain,
    cos_t,
    sin_t,
    lat_hbm,
    ctx_hbm,
    ws_hbm,
    wc_hbm,
    wg_hbm,
    proj_hbm,
    q_out,
    kv_out,
    ctx_out,
    gate_out,
    gath,
    ctx_in,
    wm,
    wj,
    modp,
    mod_sp,
    mod_all,
    modv,
    loc,
    sps,
    spr,
    tps,
    tpr,
    xs,
    xr,
    ps,
    pr,
    rs,
    rr,
    cs,
    cr,
    hs,
    hr,
):
    nx = n_tp // 2
    rows, width = gath.shape[2], gath.shape[3]
    tokens = rows * n_tp
    half = rows // 2
    mw = wm.shape[2]
    sp = lax.axis_index("sp")
    tp = lax.axis_index("tp")
    mx, core = tp // 2, lax.rem(tp, 2)
    mate = mx * 2 + 1 - core

    def x_peer(d):
        return lax.rem(mx + d, nx) * 2 + core

    loads = [
        pltpu.make_async_copy(
            lat_hbm.at[:, pl.ds(s * width, width)], gath.at[tp, s], loc.at[s]
        )
        for s in range(samples)
    ]
    mats = [
        pltpu.make_async_copy(w, wm.at[i], loc.at[samples + i])
        for i, w in enumerate((ws_hbm, wc_hbm, wg_hbm))
    ]
    joins, c0 = [], 0
    for i, w in enumerate(proj_hbm):
        joins.append(
            pltpu.make_async_copy(w, wj.at[:, pl.ds(c0, w.shape[1])], loc.at[samples + 3 + i])
        )
        c0 += w.shape[1]
    ctxs = [
        pltpu.make_async_copy(
            ctx_hbm.at[:, pl.ds(s * width, width)], ctx_in.at[s], loc.at[samples + 6 + s]
        )
        for s in range(samples)
    ]
    for c in mats + loads + ctxs + joins:
        c.start()
    enter(
        [{"tp": lax.rem(tp + d, n_tp)} for d in range(1, n_tp)]
        + [{"sp": lax.rem(sp + d, n_sp)} for d in range(1, n_sp)]
    )

    def x_send(d, s, h):
        piece = gath.at[tp, s, pl.ds(h * half, half)]
        return remote(piece, piece, xs.at[d, s, h], xr.at[d, s, h], {"tp": x_peer(d)})

    def mate_send(s):
        return remote(gath.at[tp, s], gath.at[tp, s], ps.at[s], pr.at[s], {"tp": mate})

    def relay(d, s):
        owner = lax.rem(mx - d + nx, nx) * 2 + core
        return remote(
            gath.at[owner, s], gath.at[owner, s], rs.at[d, s], rr.at[d, s], {"tp": mate}
        )

    for c in loads:
        c.wait()
    for d in range(1, nx):
        x_send(d, 0, 0).start()
    for c in mats:
        c.wait()
    for i in range(3):
        modp[:, i * mw : (i + 1) * mw] = jnp.dot(
            lifted[...], wm[i], preferred_element_type=F32
        )[:8]
    sp_sends = [
        remote(
            modp, mod_sp.at[d], sps.at[d], spr.at[d], {"sp": lax.rem(sp + d, n_sp)}
        )
        for d in range(1, n_sp)
    ]
    for c in sp_sends:
        c.start()
    for s in range(samples):
        mate_send(s).start()
    for c in sp_sends:
        c.wait()
    total = modp[...]
    for d in range(1, n_sp):
        total = total + mod_sp[d]
    mod_all[tp] = total
    tp_sends = [
        remote(
            mod_all.at[tp],
            mod_all.at[tp],
            tps.at[d],
            tpr.at[d],
            {"tp": lax.rem(tp + d, n_tp)},
        )
        for d in range(1, n_tp)
    ]
    for c in tp_sends:
        c.start()
    for s in range(samples):
        for h in range(2):
            if s or h:
                for d in range(1, nx):
                    x_send(d, s, h).start()
    for c in tp_sends:
        c.wait()
    for t in range(n_tp):
        for i in range(3):
            modv[:, i * width + t * mw : i * width + (t + 1) * mw] = mod_all[
                t, :, i * mw : (i + 1) * mw
            ]
    gate_out[...] = modv[:, 2 * width :]
    modv[:, width : 2 * width] = gain[...] * (1.0 + modv[:, width : 2 * width])

    def norm(block, row):
        up = block.astype(F32)
        inv = lax.rsqrt(jnp.mean(up * up, axis=-1, keepdims=True) + EPS)
        return (
            up * inv * modv[pl.ds(row, 1), width : 2 * width] + modv[pl.ds(row, 1), :width]
        ).astype(BF16)

    for c in joins + ctxs:
        c.wait()

    def ctx_step(s, carry):
        ctx_out[sp, s] = jnp.dot(
            norm(ctx_in[s], samples), wj[:, q_cols:], preferred_element_type=F32
        ).astype(BF16)
        return carry

    lax.fori_loop(0, samples, ctx_step, 0)
    ctx_sends = [
        remote(
            ctx_out.at[sp], ctx_out.at[sp], cs.at[d], cr.at[d], {"sp": lax.rem(sp + d, n_sp)}
        )
        for d in range(1, n_sp)
    ]
    for c in ctx_sends:
        c.start()
    scale = HEAD_DIM**-0.5
    lane = lax.broadcasted_iota(jnp.int32, (rows, 128), 1)
    low = lax.rem(lane, HEAD_DIM) < HEAD_DIM // 2

    def project(owner, s):
        at = pl.multiple_of(owner * rows, rows)
        out = jnp.dot(norm(gath[owner, s], s), wj[...], preferred_element_type=F32)
        cosine = cos_t[pl.ds(at, rows), :]
        sine = sin_t[pl.ds(at, rows), :]
        for c0 in range(0, q_cols + 2 * kv_cols, 128):
            part = out[:, c0 : c0 + 128]
            turned = part
            if c0 < q_cols + kv_cols:
                swapped = jnp.where(low, pltpu.roll(part, 96, 1), pltpu.roll(part, 32, 1))
                turned = part * cosine + swapped * sine
            if c0 < q_cols:
                q_out[s, pl.ds(at, rows), c0 : c0 + 128] = (turned * scale).astype(BF16)
            else:
                if c0 + 128 > q_cols + kv_cols and c0 < q_cols + kv_cols:
                    turned = jnp.where(lane < q_cols + kv_cols - c0, turned, part)
                kv_out[s, pl.ds(WINDOW + at, rows), c0 - q_cols : c0 - q_cols + 128] = (
                    turned.astype(BF16)
                )

    def own_step(s, carry):
        project(tp, s)
        return carry

    lax.fori_loop(0, samples, own_step, 0)

    def mate_step(s, carry):
        mate_send(s).wait_recv()
        project(mate, s)
        return carry

    lax.fori_loop(0, samples, mate_step, 0)

    def x_step(s, carry):
        for d in range(1, nx):
            for h in range(2):
                x_send(d, s, h).wait_recv()
            relay(d, s).start()
        for d in range(1, nx):
            project(lax.rem(mx - d + nx, nx) * 2 + core, s)
        for d in range(1, nx):
            relay(d, s).wait_recv()
            project(lax.rem(mx - d + nx, nx) * 2 + 1 - core, s)
        return carry

    up_edge = sp == n_sp - 1
    down_edge = sp == 0

    def halo_up():
        return remote(
            kv_out.at[:, pl.ds(tokens, WINDOW)],
            kv_out.at[:, pl.ds(0, WINDOW)],
            hs.at[0],
            hr.at[0],
            {"sp": lax.rem(sp + 1, n_sp)},
        )

    def halo_down():
        return remote(
            kv_out.at[:, pl.ds(WINDOW, WINDOW)],
            kv_out.at[:, pl.ds(tokens + WINDOW, WINDOW)],
            hs.at[1],
            hr.at[1],
            {"sp": lax.rem(sp + n_sp - 1, n_sp)},
        )

    lax.fori_loop(0, samples, x_step, 0)
    zero = jnp.zeros((samples, WINDOW, 2 * kv_cols), BF16)

    @pl.when(jnp.logical_not(up_edge))
    def _():
        halo_up().start()

    @pl.when(jnp.logical_not(down_edge))
    def _():
        halo_down().start()

    @pl.when(up_edge)
    def _():
        kv_out[:, tokens + WINDOW :, :] = zero

    @pl.when(down_edge)
    def _():
        kv_out[:, :WINDOW, :] = zero

    for c in ctx_sends:
        c.wait()
    for s in range(samples):
        mate_send(s).wait_send()
        for d in range(1, nx):
            for h in range(2):
                x_send(d, s, h).wait_send()
            relay(d, s).wait_send()

    @pl.when(jnp.logical_not(up_edge))
    def _():
        halo_up().wait_send()
        halo_down().wait_recv()

    @pl.when(jnp.logical_not(down_edge))
    def _():
        halo_down().wait_send()
        halo_up().wait_recv()


def attend_kernel(n_sp, kv_cols, per_group, sinks, q_ref, kv_ref, ctx_ref, out_ref):
    s = pl.program_id(0)
    block = pl.program_id(1)
    rows = q_ref.shape[1]
    span = rows + 2 * WINDOW
    tokens = kv_ref.shape[1] - 2 * WINDOW
    sp = lax.axis_index("sp")
    at = pl.multiple_of(block * rows, rows)
    window = kv_ref[0, pl.ds(at, span), :]
    ctx = ctx_ref[:, 0].reshape(-1, 2 * kv_cols)
    stacked = per_group * rows
    row = lax.rem(lax.broadcasted_iota(jnp.int32, (stacked, span), 0), rows)
    col = lax.broadcasted_iota(jnp.int32, (stacked, span), 1)
    k_pos = sp * tokens + at - WINDOW + col
    keep = (col >= row) & (col <= row + 2 * WINDOW) & (k_pos >= 0) & (k_pos < n_sp * tokens)
    first = lax.broadcasted_iota(jnp.int32, (stacked, 1), 0)
    contract = (((1,), (1,)), ((), ()))
    for g in range(kv_cols // HEAD_DIM):
        q = jnp.concatenate(
            [
                q_ref[0, :, (g * per_group + j) * HEAD_DIM : (g * per_group + j + 1) * HEAD_DIM]
                for j in range(per_group)
            ],
            axis=0,
        )
        sink = jnp.full((stacked, 1), sinks[g * per_group], F32)
        for j in range(1, per_group):
            sink = jnp.where(first >= j * rows, sinks[g * per_group + j], sink)
        ks = slice(g * HEAD_DIM, (g + 1) * HEAD_DIM)
        vs = slice(kv_cols + g * HEAD_DIM, kv_cols + (g + 1) * HEAD_DIM)
        near = lax.dot_general(q, window[:, ks], contract, preferred_element_type=F32)
        near = jnp.where(keep, near, BIG_NEG)
        far = lax.dot_general(q, ctx[:, ks], contract, preferred_element_type=F32)
        top = jnp.maximum(
            jnp.maximum(
                jnp.max(near, axis=-1, keepdims=True), jnp.max(far, axis=-1, keepdims=True)
            ),
            sink,
        )
        near = jnp.exp(near - top)
        far = jnp.exp(far - top)
        below = (
            jnp.sum(near, axis=-1, keepdims=True)
            + jnp.sum(far, axis=-1, keepdims=True)
            + jnp.exp(sink - top)
        )
        total = jnp.dot(near.astype(BF16), window[:, vs], preferred_element_type=F32)
        total = total + jnp.dot(far.astype(BF16), ctx[:, vs], preferred_element_type=F32)
        total = (total / below).astype(BF16)
        for j in range(per_group):
            h = g * per_group + j
            out_ref[0, :, h * HEAD_DIM : (h + 1) * HEAD_DIM] = total[j * rows : (j + 1) * rows]


def back_kernel(
    n_tp,
    samples,
    att,
    w_out,
    gate,
    lat,
    out,
    acc,
    dsend,
    drecv,
    xsend,
    xrecv,
    ds_,
    dr_,
    xs,
    xr,
):
    nx = n_tp // 2
    rows, width = acc.shape[1], acc.shape[2]
    tp = lax.axis_index("tp")
    mx, core = tp // 2, lax.rem(tp, 2)
    mate = {"tp": mx * 2 + 1 - core}
    enter([mate] + [{"tp": lax.rem(mx + d, nx) * 2 + core} for d in range(1, nx)])

    def product(d, s, side):
        at = pl.multiple_of((lax.rem(mx + d, nx) * 2 + side) * rows, rows)
        return jnp.dot(att[s, pl.ds(at, rows), :], w_out[...], preferred_element_type=F32)

    def to_mate(d, s):
        return remote(dsend.at[d, s], drecv.at[d, s], ds_.at[d, s], dr_.at[d, s], mate)

    def across(d, s):
        peer = {"tp": lax.rem(mx + d, nx) * 2 + core}
        return remote(xsend.at[d, s], xrecv.at[d, s], xs.at[d, s], xr.at[d, s], peer)

    def step(i, carry):
        d = lax.rem(1 + i // samples, nx)
        s = lax.rem(i, samples)
        dsend[d, s] = product(d, s, 1 - core).astype(BF16)
        to_mate(d, s).start()
        mine = product(d, s, core)
        to_mate(d, s).wait()
        mine = mine + drecv[d, s].astype(F32)

        @pl.when(i < (nx - 1) * samples)
        def _():
            xsend[d, s] = mine.astype(BF16)
            across(d, s).start()

        @pl.when(i >= (nx - 1) * samples)
        def _():
            acc[s] = mine

        return carry

    lax.fori_loop(0, nx * samples, step, 0)
    for s in range(samples):
        for d in range(1, nx):
            across(d, s).wait()
        mixed = acc[s]
        for d in range(1, nx):
            mixed = mixed + xrecv[d, s].astype(F32)
        cols = slice(s * width, (s + 1) * width)
        out[:, cols] = (lat[:, cols].astype(F32) + gate[s : s + 1, :] * mixed).astype(BF16)


def on_device(
    latents,
    context,
    condition,
    cond_context,
    w_shift,
    w_scale,
    w_gate,
    norm_gain,
    w_query,
    w_key,
    w_value,
    sink_logit,
    w_out,
):
    rows, samples, width = latents.shape
    n_tp = lax.axis_size("tp")
    n_sp = lax.axis_size("sp")
    nx = n_tp // 2
    tokens = rows * n_tp
    q_cols = w_query.shape[1]
    kv_cols = w_key.shape[1]
    ctx_rows = context.shape[0]
    per_group = q_cols // kv_cols
    mod_rows, mw = w_shift.shape
    lifted = jax.nn.silu(jnp.concatenate([condition, cond_context[None, :]], axis=0)).astype(BF16)
    lifted = jnp.pad(lifted, ((0, 16 - samples - 1), (0, 0)))
    offset = lax.axis_index("sp") * tokens
    positions = offset + jnp.arange(tokens, dtype=jnp.int32)
    quarter = HEAD_DIM // 4
    inverse = THETA ** (-jnp.arange(quarter, dtype=F32) / quarter)
    grid_row = (positions // GRID_W).astype(F32)
    grid_col = (positions % GRID_W).astype(F32)
    angles = jnp.concatenate([grid_row[:, None] * inverse, grid_col[:, None] * inverse], axis=-1)
    cosine, sine = jnp.cos(angles), jnp.sin(angles)
    cos_t = jnp.concatenate([cosine] * 4, axis=-1)
    sin_t = jnp.concatenate([-sine, sine, -sine, sine], axis=-1)
    flat = latents.reshape(rows, samples * width)
    flat_ctx = context.reshape(ctx_rows, samples * width)
    if kv_cols % 128:
        projections = (w_query, jnp.concatenate([w_key, w_value], axis=1))
    else:
        projections = (w_query, w_key, w_value)
    dma = pltpu.SemaphoreType.DMA
    q, kv, ctx, gate = pl.pallas_call(
        functools.partial(front_kernel, n_tp, n_sp, samples, q_cols, kv_cols),
        out_shape=(
            jax.ShapeDtypeStruct((samples, tokens, q_cols), BF16),
            jax.ShapeDtypeStruct((samples, tokens + 2 * WINDOW, 2 * kv_cols), BF16),
            jax.ShapeDtypeStruct((n_sp, samples, ctx_rows, 2 * kv_cols), BF16),
            jax.ShapeDtypeStruct((8, width), F32),
        ),
        in_specs=[VMEM] * 4 + [ANY] * (5 + len(projections)),
        out_specs=(VMEM,) * 4,
        scratch_shapes=[
            pltpu.VMEM((n_tp, samples, rows, width), BF16),
            pltpu.VMEM((samples, ctx_rows, width), BF16),
            pltpu.VMEM((3, mod_rows, mw), BF16),
            pltpu.VMEM((width, q_cols + 2 * kv_cols), BF16),
            pltpu.VMEM((8, 3 * mw), F32),
            pltpu.VMEM((n_sp, 8, 3 * mw), F32),
            pltpu.VMEM((n_tp, 8, 3 * mw), F32),
            pltpu.VMEM((8, 3 * width), F32),
            dma((2 * samples + 6,)),
            dma((n_sp,)),
            dma((n_sp,)),
            dma((n_tp,)),
            dma((n_tp,)),
            dma((nx, samples, 2)),
            dma((nx, samples, 2)),
            dma((samples,)),
            dma((samples,)),
            dma((nx, samples)),
            dma((nx, samples)),
            dma((n_sp,)),
            dma((n_sp,)),
            dma((2,)),
            dma((2,)),
        ],
        compiler_params=pltpu.CompilerParams(
            collective_id=0, has_side_effects=True, vmem_limit_bytes=VMEM_LIMIT
        ),
        name="front",
    )(
        lifted,
        norm_gain.reshape(1, width),
        cos_t,
        sin_t,
        flat,
        flat_ctx,
        w_shift,
        w_scale,
        w_gate,
        *projections,
    )
    block = min(tokens, 128)
    att = pl.pallas_call(
        functools.partial(attend_kernel, n_sp, kv_cols, per_group),
        grid=(samples, tokens // block),
        out_shape=jax.ShapeDtypeStruct((samples, tokens, q_cols), BF16),
        in_specs=[
            pl.BlockSpec(memory_space=pltpu.SMEM),
            pl.BlockSpec((1, block, q_cols), lambda s, b: (s, b, 0)),
            pl.BlockSpec((1, tokens + 2 * WINDOW, 2 * kv_cols), lambda s, b: (s, 0, 0)),
            pl.BlockSpec((n_sp, 1, ctx_rows, 2 * kv_cols), lambda s, b: (0, s, 0, 0)),
        ],
        out_specs=pl.BlockSpec((1, block, q_cols), lambda s, b: (s, b, 0)),
        compiler_params=pltpu.CompilerParams(vmem_limit_bytes=VMEM_LIMIT),
        name="attend",
    )(sink_logit, q, kv, ctx)
    out = pl.pallas_call(
        functools.partial(back_kernel, n_tp, samples),
        out_shape=jax.ShapeDtypeStruct((rows, samples * width), BF16),
        in_specs=[VMEM] * 4,
        out_specs=VMEM,
        scratch_shapes=[
            pltpu.VMEM((samples, rows, width), F32),
            pltpu.VMEM((nx, samples, rows, width), BF16),
            pltpu.VMEM((nx, samples, rows, width), BF16),
            pltpu.VMEM((nx, samples, rows, width), BF16),
            pltpu.VMEM((nx, samples, rows, width), BF16),
            dma((nx, samples)),
            dma((nx, samples)),
            dma((nx, samples)),
            dma((nx, samples)),
        ],
        compiler_params=pltpu.CompilerParams(
            collective_id=1, has_side_effects=True, vmem_limit_bytes=VMEM_LIMIT
        ),
        name="back",
    )(att, w_out, gate, flat)
    return out.reshape(rows, samples, width)


def solution(mesh):
    return jax.shard_map(
        on_device,
        mesh=mesh,
        in_specs=(
            P(("sp", "tp"), "grp", None),
            P("sp", "grp", None),
            P("grp", "sp"),
            P("sp"),
            P("sp", "tp"),
            P("sp", "tp"),
            P("sp", "tp"),
            P(),
            P(None, "tp"),
            P(None, "tp"),
            P(None, "tp"),
            P("tp"),
            P("tp", None),
        ),
        out_specs=P(("sp", "tp"), "grp", None),
        check_vma=False,
    )
```

time: 239 us -> 99.9 us (0.42); the launches traced: 236 us -> 99.6 us
  Pallas kernels: 0 us -> 89.3 us
  waiting for transfers between devices: 89.3 us -> 0 us
  matrix products: 37.3 us -> 0 us
  blocking collectives: 32.3 us -> 0 us
  other arithmetic: 27.7 us -> 3.15 us
  local copies, waits for them, and re-layouts: 30.5 us -> 7.05 us
  between operations: 13.4 us -> 0.07 us
  starting transfers between devices: 5.55 us -> 0 us
    pallas_call x0 -> x3, Pallas kernels: none -> 89.3 us  [the longest x1 44.6 us: on_device(): pl.pallas_call(functools.partial(front_kernel, n_tp, n_sp, samples, q_col...]
    all_gather x2 -> x0, waiting for transfers between devices: 51.3 us -> none  [the longest x1 31.5 us: on_device(): shard_rows = lax.all_gather(normed, 'tp', axis=0, tiled=True)]
    reduce_scatter x1 -> x0, waiting for transfers between devices: 37.9 us -> none  [on_device(): lax.psum_scatter(jnp.dot(attended, w_out, preferred_element_type=jnp.floa...]
    dot_general x10 -> x0, matrix products: 37.3 us -> none  [the longest x1 8.13 us: attend_block(): jnp.einsum('qsngd,ksnd->sngqk', q_blk, ctx_keys, preferred_element_type=j...]
    all_gather x3 -> x0, blocking collectives: 20.2 us -> none  [the longest x1 9.18 us: on_device(): lax.all_gather(sum_shift, 'tp', axis=1, tiled=True)]
    reduce_sum x4 -> x0, other arithmetic: 16.2 us -> none  [the longest x1 9.31 us: attend_block(): jnp.sum(ctx_exp, axis=-1)]
    psum x1 -> x0, blocking collectives: 12.1 us -> none  [on_device(): lax.psum((part_shift, part_scale, part_gate), 'sp')]
    reshape x4 -> x1, local copies, waits for them, and re-layouts: 11.1 us -> 2.62 us  [on_device(): return out.reshape(rows, samples, width)]
  transfers between devices with their start and end apart: 5 -> 0, of which waited for: 3 -> 0; matrix products, arithmetic and copies ran while one was open for 9% -> 0% of each run, Pallas kernels for 0% -> 0%
where the time goes in v1:
time: 99.9 us; the launch traced here: 99.6 us
  Pallas kernels  89.3 us (89%)
  local copies, waits for them, and re-layouts  7.05 us (7%)
  other arithmetic  3.15 us (3%)
    pallas_call x1, Pallas kernels, on_device(): pl.pallas_call(functools.partial(front_kernel, n_tp, n_sp, samples, q_col...  44.6 us
    pallas_call x1, Pallas kernels, on_device(): pl.pallas_call(functools.partial(back_kernel, n_tp, samples), out_shape=j...  30.6 us
    pallas_call x1, Pallas kernels, on_device(): pl.pallas_call(functools.partial(attend_kernel, n_sp, kv_cols, per_group)...  14.2 us
    unnamed x6, local copies, waits for them, and re-layouts  3.58 us
    reshape x1, local copies, waits for them, and re-layouts, on_device(): return out.reshape(rows, samples, width)  2.62 us

profile of v1, /device:TPU:13, one launch (start us, length us, event | category | flops | bytes accessed | tf_op | source)
XLA Modules:
  0.0 99.6 jit_solution(5330851930777363604)
XLA Ops:
  0.0 0.0 copy-start.1
  0.0 0.8 fusion.2
  0.8 0.6 pad.4.lifted
  1.5 0.1 broadcast_multiply_fusion.1
  1.5 0.2 fusion
  1.8 0.1 copy.20
  1.9 0.0 copy-start
  1.9 1.0 pad_maximum_fusion.1.sin_t
  2.9 0.1 copy.16
  3.1 1.0 %pad_maximum_fusion.cos_t = f32[512,128]{1,0:T(8,128)} fusion(f32[512,32]{1,0:T(8,128)S(1)} %copy.16), kind=kLoop, calls=%fused_computation | loop fusion | flops 196608 | bytes 327680 | tf_op jit(solution)/shard_map/concatenate | solution.py:510
  4.1 0.0 copy-done.1
  4.1 1.3 %copy.23 = bf16[16,8,2,2048]{3,1,2,0:T(8,128)(2,1)} copy(bf16[16,8,2,2048]{3,2,1,0:T(2,128)(2,1)S(1)} %bitcast.10) | data formatting | bytes 2097152
  5.4 0.0 copy-done
  5.4 2.2 %copy.24 = bf16[32,8,2,2048]{3,1,2,0:T(8,128)(2,1)} copy(bf16[32,8,2,2048]{3,2,1,0:T(2,128)(2,1)S(1)} %bitcast.9) | data formatting | bytes 4194304
  7.6 44.6 %front.1 = (bf16[2,512,256]{2,1,0:T(8,128)(2,1)}, bf16[2,768,256]{2,1,0:T(8,128)(2,1)}, bf16[4,2,256,256]{3,2,1,0:T(8,128)(2,1)}, f32[8,2048]{1,0:T(8,128)}) custom-call(bf16[16,512]{1,0:T(8,128)(2,1)} %pad.4.lifted, f32[1,2048]{1,0:T(1,128)} %bitcast.11, f32[512,128]{1,0:T(8,128)} %pad_maximum_fusion.cos_t, f32[512,128]{1,0:T(8,128)} %pad_maximum_fusion.1.sin_t, ...), custom_call_target="tpu_custom_call" | custom-call | tf_op jit(solution)/shard_map/front/pallas_call | solution.py:519
  52.2 14.2 %attend.1.att = bf16[2,512,256]{2,1,0:T(8,128)(2,1)} custom-call(f32[4]{0:T(128)} %sinks.1, bf16[2,512,256]{2,1,0:T(8,128)(2,1)} %get-tuple-element.9.q_ref, bf16[2,768,256]{2,1,0:T(8,128)(2,1)} %get-tuple-element.10.kv_ref, bf16[4,2,256,256]{3,2,1,0:T(8,128)(2,1)} %get-tuple-element.11.ctx_ref), custom_call_target="tpu_custom_call" | custom-call | tf_op jit(solution)/shard_map/attend/pallas_call | solution.py:571
  66.4 30.6 %back.1 = bf16[128,4096]{1,0:T(8,128)(2,1)} custom-call(bf16[2,512,256]{2,1,0:T(8,128)(2,1)} %attend.1.att, bf16[256,2048]{1,0:T(8,128)(2,1)} %w_out.1, f32[8,2048]{1,0:T(8,128)} %get-tuple-element.12.gate, bf16[128,4096]{1,0:T(8,128)(2,1)} %bitcast.7), custom_call_target="tpu_custom_call" | custom-call | tf_op jit(solution)/shard_map/back/pallas_call | solution.py:585
  97.0 2.6 %reshape.55 = bf16[128,2,2048]{2,1,0:T(2,128)(2,1)} reshape(bf16[128,4096]{1,0:T(8,128)(2,1)} %back.1) | data formatting | bytes 2097152 | tf_op jit(solution)/shard_map/reshape | solution.py:606
  (3 shorter events, 0.0 us)
Async XLA Ops:
  0.0 4.1 %copy-start.1 = (bf16[128,2,2048]{2,1,0:T(2,128)(2,1)S(1)}, bf16[128,2,2048]{2,1,0:T(2,128)(2,1)}, u32[]{:S(2)}) copy-start(bf16[128,2,2048]{2,1,0:T(2,128)(2,1)} %param.13) | copy-start | bytes 3145732
  1.9 3.5 %copy-start = (bf16[256,2,2048]{2,1,0:T(2,128)(2,1)S(1)}, bf16[256,2,2048]{2,1,0:T(2,128)(2,1)}, u32[]{:S(2)}) copy-start(bf16[256,2,2048]{2,1,0:T(2,128)(2,1)} %param.14) | copy-start | bytes 6291460

commit v2 on v0

v2 whole, which is shorter than its diff:
```python
import functools

import jax
import jax.numpy as jnp
import numpy as np
from jax import lax
from jax.experimental import pallas as pl
from jax.experimental.pallas import tpu as pltpu
from jax.sharding import PartitionSpec as P

HEAD_DIM = 64
WINDOW = 128
GRID_W = 64
EPS = 1e-06
THETA = 10000.0
BIG_NEG = -1e30
VMEM_LIMIT = 60 * 1024 * 1024
F32 = jnp.float32
BF16 = jnp.bfloat16
ANY = pl.BlockSpec(memory_space=pl.ANY)
VMEM = pl.BlockSpec(memory_space=pltpu.VMEM)


def enter(peers):
    barrier = pltpu.get_barrier_semaphore()
    for peer in peers:
        pl.semaphore_signal(
            barrier, inc=1, device_id=peer, device_id_type=pl.DeviceIdType.MESH
        )
    pl.semaphore_wait(barrier, len(peers))


def remote(src, dst, send, recv, peer):
    return pltpu.make_async_remote_copy(
        src_ref=src,
        dst_ref=dst,
        send_sem=send,
        recv_sem=recv,
        device_id=peer,
        device_id_type=pl.DeviceIdType.MESH,
    )


def block_kernel(n_tp, n_sp, samples, q_cols, kv_cols, n_proj, *refs):
    cond, cond_ctx, gain, cos_row, sin_row, cos_col, sin_col, sinks = refs[:8]
    lat_hbm, ctx_hbm, ws_hbm, wc_hbm, wg_hbm, wo_hbm = refs[8:14]
    proj_hbm = refs[14 : 14 + n_proj]
    out = refs[14 + n_proj]
    (
        gath,
        ctx_in,
        wm,
        wj,
        wo,
        modp,
        mod_sp,
        mod_all,
        modv,
        cos_t,
        sin_t,
        queries,
        kv,
        ctx_all,
        att,
        arr,
        loc,
        sps,
        spr,
        tps,
        tpr,
        xs,
        xr,
        ps,
        pr,
        rs,
        rr,
        cs,
        cr,
        hs,
        hr,
        avs,
        avr,
    ) = refs[15 + n_proj :]
    nx = n_tp // 2
    rows, width = gath.shape[2], gath.shape[3]
    tokens = rows * n_tp
    mw = wm.shape[2]
    per_group = q_cols // kv_cols
    sp = lax.axis_index("sp")
    tp = lax.axis_index("tp")
    mx, core = tp // 2, lax.rem(tp, 2)
    mate = {"tp": mx * 2 + 1 - core}
    pieces = wo.shape[1]
    wo_rows = wo.shape[2]

    def local(i, src, dst):
        return pltpu.make_async_copy(src, dst, loc.at[i])

    n_loc = 0
    loads, mats, joins, ctxs, outs = [], [], [], [], []
    for s in range(samples):
        loads.append(local(n_loc, lat_hbm.at[:, pl.ds(s * width, width)], gath.at[tp, s]))
        n_loc += 1
    for i, w in enumerate((ws_hbm, wc_hbm, wg_hbm)):
        mats.append(local(n_loc, w, wm.at[i]))
        n_loc += 1
    for s in range(samples):
        ctxs.append(local(n_loc, ctx_hbm.at[:, pl.ds(s * width, width)], ctx_in.at[s]))
        n_loc += 1
    c0 = 0
    for w in proj_hbm:
        joins.append(local(n_loc, w, wj.at[:, pl.ds(c0, w.shape[1])]))
        c0 += w.shape[1]
        n_loc += 1
    for i in range(pieces):
        outs.append(local(n_loc, wo_hbm.at[pl.ds(i * wo_rows, wo_rows)], wo.at[tp, i]))
        n_loc += 1
    for c in loads + mats + ctxs + joins + outs:
        c.start()
    enter(
        [{"tp": lax.rem(tp + d, n_tp)} for d in range(1, n_tp)]
        + [{"sp": lax.rem(sp + d, n_sp)} for d in range(1, n_sp)]
    )

    def spot(owner, i, kind):
        return (wo if kind else gath).at[owner, i]

    def x_send(d, i, kind=0):
        peer = {"tp": lax.rem(mx + d, nx) * 2 + core}
        at = i + kind * samples
        piece = spot(tp, i, kind)
        return remote(piece, piece, xs.at[d, at], xr.at[d, at], peer)

    def mate_send(i, kind=0):
        at = i + kind * samples
        piece = spot(tp, i, kind)
        return remote(piece, piece, ps.at[at], pr.at[at], mate)

    def relay(d, i, kind=0):
        at = i + kind * samples
        piece = spot(lax.rem(mx - d + nx, nx) * 2 + core, i, kind)
        return remote(piece, piece, rs.at[d, at], rr.at[d, at], mate)

    for c in loads:
        c.wait()
    for d in range(1, nx):
        x_send(d, 0).start()
    given = jnp.concatenate(
        [cond[...], cond_ctx[...], jnp.zeros((16 - samples - 1, cond.shape[1]), F32)], axis=0
    )
    lifted = (given / (1.0 + jnp.exp(-given))).astype(BF16)
    for c in mats:
        c.wait()
    for i in range(3):
        part = jnp.dot(lifted, wm[i], preferred_element_type=F32)
        for r in range(samples + 1):
            modp[r, :, i * mw : (i + 1) * mw] = part[r : r + 1]
    sp_sends = [
        remote(modp, mod_sp.at[d], sps.at[d], spr.at[d], {"sp": lax.rem(sp + d, n_sp)})
        for d in range(1, n_sp)
    ]
    for c in sp_sends:
        c.start()
    for s in range(samples):
        mate_send(s).start()
    line = tokens // GRID_W
    axis_row = lax.rem(lax.broadcasted_iota(jnp.int32, (GRID_W, 128), 1), 32) < HEAD_DIM // 4
    for r in range(line):
        cos_t[r * GRID_W : (r + 1) * GRID_W] = jnp.where(
            axis_row, cos_row[pl.ds(sp * line + r, 1), :], cos_col[...]
        )
        sin_t[r * GRID_W : (r + 1) * GRID_W] = jnp.where(
            axis_row, sin_row[pl.ds(sp * line + r, 1), :], sin_col[...]
        )
    for c in sp_sends:
        c.wait()
    total = modp[...]
    for d in range(1, n_sp):
        total = total + mod_sp[d]
    mod_all[tp] = total
    tp_sends = [
        remote(
            mod_all.at[tp],
            mod_all.at[tp],
            tps.at[d],
            tpr.at[d],
            {"tp": lax.rem(tp + d, n_tp)},
        )
        for d in range(1, n_tp)
    ]
    for c in tp_sends:
        c.start()
    for s in range(1, samples):
        for d in range(1, nx):
            x_send(d, s).start()
    for c in outs:
        c.wait()
    for i in range(pieces):
        for d in range(1, nx):
            x_send(d, i, 1).start()
        mate_send(i, 1).start()
    for c in tp_sends:
        c.wait()
    for t in range(n_tp):
        for i in range(3):
            modv[:, :, i * width + t * mw : i * width + (t + 1) * mw] = mod_all[
                t, :, :, i * mw : (i + 1) * mw
            ]
    for r in range(samples + 1):
        modv[r, :, width : 2 * width] = gain[...] * (1.0 + modv[r, :, width : 2 * width])

    def norm(block, row):
        up = block.astype(F32)
        inv = lax.rsqrt(jnp.mean(up * up, axis=-1, keepdims=True) + EPS)
        return (up * inv * modv[row, :, width : 2 * width] + modv[row, :, :width]).astype(BF16)

    for c in joins + ctxs:
        c.wait()

    def ctx_step(s, carry):
        ctx_all[sp, s] = jnp.dot(
            norm(ctx_in[s], samples), wj[:, q_cols:], preferred_element_type=F32
        ).astype(BF16)
        return carry

    lax.fori_loop(0, samples, ctx_step, 0)
    ctx_sends = [
        remote(
            ctx_all.at[sp], ctx_all.at[sp], cs.at[d], cr.at[d], {"sp": lax.rem(sp + d, n_sp)}
        )
        for d in range(1, n_sp)
    ]
    for c in ctx_sends:
        c.start()
    scale = HEAD_DIM**-0.5
    lane = lax.broadcasted_iota(jnp.int32, (rows, 128), 1)
    low = lax.rem(lane, HEAD_DIM) < HEAD_DIM // 2

    def project(owner, s):
        at = pl.multiple_of(owner * rows, rows)
        res = jnp.dot(norm(gath[owner, s], s), wj[...], preferred_element_type=F32)
        cosine = cos_t[pl.ds(at, rows), :]
        sine = sin_t[pl.ds(at, rows), :]
        for c0 in range(0, q_cols + 2 * kv_cols, 128):
            part = res[:, c0 : c0 + 128]
            turned = part
            if c0 < q_cols + kv_cols:
                swapped = jnp.where(low, pltpu.roll(part, 96, 1), pltpu.roll(part, 32, 1))
                turned = part * cosine + swapped * sine
            if c0 < q_cols:
                queries[s, pl.ds(at, rows), c0 : c0 + 128] = (turned * scale).astype(BF16)
            else:
                if c0 + 128 > q_cols + kv_cols and c0 < q_cols + kv_cols:
                    turned = jnp.where(lane < q_cols + kv_cols - c0, turned, part)
                kv[s, pl.ds(WINDOW + at, rows), c0 - q_cols : c0 - q_cols + 128] = turned.astype(
                    BF16
                )

    up_edge = sp == n_sp - 1
    down_edge = sp == 0

    def halo_up(s):
        return remote(
            kv.at[s, pl.ds(tokens, WINDOW)],
            kv.at[s, pl.ds(0, WINDOW)],
            hs.at[0, s],
            hr.at[0, s],
            {"sp": lax.rem(sp + 1, n_sp)},
        )

    def halo_down(s):
        return remote(
            kv.at[s, pl.ds(WINDOW, WINDOW)],
            kv.at[s, pl.ds(tokens + WINDOW, WINDOW)],
            hs.at[1, s],
            hr.at[1, s],
            {"sp": lax.rem(sp + n_sp - 1, n_sp)},
        )

    zero = jnp.zeros((WINDOW, 2 * kv_cols), BF16)

    def sample_step(s, carry):
        def own_and_mate(k, inner):
            @pl.when(k == 1)
            def _():
                mate_send(s).wait_recv()

            project(lax.rem(tp + 0, n_tp) * (1 - k) + (mx * 2 + 1 - core) * k, s)
            return inner

        lax.fori_loop(0, 2, own_and_mate, 0)
        for d in range(1, nx):
            x_send(d, s).wait_recv()
            relay(d, s).start()

        def crossed(k, inner):
            d = 1 + k // 2
            far = lax.rem(k, 2)

            @pl.when(far == 1)
            def _():
                relay(d, s).wait_recv()

            side = core * (1 - far) + (1 - core) * far
            project(lax.rem(mx - d + nx, nx) * 2 + side, s)
            return inner

        lax.fori_loop(0, 2 * (nx - 1), crossed, 0)

        @pl.when(jnp.logical_not(up_edge))
        def _():
            halo_up(s).start()

        @pl.when(jnp.logical_not(down_edge))
        def _():
            halo_down(s).start()

        @pl.when(up_edge)
        def _():
            kv[s, tokens + WINDOW :, :] = zero

        @pl.when(down_edge)
        def _():
            kv[s, :WINDOW, :] = zero

        return carry

    lax.fori_loop(0, samples, sample_step, 0)
    for c in ctx_sends:
        c.wait()
    q_rows = min(tokens, 128)
    span = q_rows + 2 * WINDOW
    stacked = per_group * q_rows
    contract = (((1,), (1,)), ((), ()))

    def attend(s, block):
        at = pl.multiple_of(block * q_rows, q_rows)
        window = kv[s, pl.ds(at, span), :]
        ctx = ctx_all[:, s].reshape(-1, 2 * kv_cols)
        q_all = queries[s, pl.ds(at, q_rows), :]
        row = lax.rem(lax.broadcasted_iota(jnp.int32, (stacked, span), 0), q_rows)
        col = lax.broadcasted_iota(jnp.int32, (stacked, span), 1)
        k_pos = sp * tokens + at - WINDOW + col
        keep = (col >= row) & (col <= row + 2 * WINDOW) & (k_pos >= 0) & (k_pos < n_sp * tokens)
        first = lax.broadcasted_iota(jnp.int32, (stacked, 1), 0)
        for g in range(kv_cols // HEAD_DIM):
            heads = range(g * per_group, (g + 1) * per_group)
            q = jnp.concatenate(
                [q_all[:, h * HEAD_DIM : (h + 1) * HEAD_DIM] for h in heads], axis=0
            )
            sink = jnp.full((stacked, 1), sinks[g * per_group], F32)
            for j in range(1, per_group):
                sink = jnp.where(first >= j * q_rows, sinks[g * per_group + j], sink)
            ks = slice(g * HEAD_DIM, (g + 1) * HEAD_DIM)
            vs = slice(kv_cols + g * HEAD_DIM, kv_cols + (g + 1) * HEAD_DIM)
            near = lax.dot_general(q, window[:, ks], contract, preferred_element_type=F32)
            near = jnp.where(keep, near, BIG_NEG)
            far = lax.dot_general(q, ctx[:, ks], contract, preferred_element_type=F32)
            top = jnp.maximum(
                jnp.maximum(
                    jnp.max(near, axis=-1, keepdims=True), jnp.max(far, axis=-1, keepdims=True)
                ),
                sink,
            )
            near = jnp.exp(near - top)
            far = jnp.exp(far - top)
            below = (
                jnp.sum(near, axis=-1, keepdims=True)
                + jnp.sum(far, axis=-1, keepdims=True)
                + jnp.exp(sink - top)
            )
            mixed = jnp.dot(near.astype(BF16), window[:, vs], preferred_element_type=F32)
            mixed = mixed + jnp.dot(far.astype(BF16), ctx[:, vs], preferred_element_type=F32)
            mixed = (mixed / below).astype(BF16)
            for j, h in enumerate(heads):
                att[s, pl.ds(at, q_rows), h * HEAD_DIM : (h + 1) * HEAD_DIM] = mixed[
                    j * q_rows : (j + 1) * q_rows
                ]

    def swap(d, s):
        to = lax.rem(tp + d, n_tp)
        at = pl.multiple_of(to * rows, rows)
        return remote(
            att.at[s, pl.ds(at, rows)], arr.at[s, tp], avs.at[d, s], avr.at[d, s], {"tp": to}
        )

    def attend_step(s, carry):
        @pl.when(jnp.logical_not(down_edge))
        def _():
            halo_up(s).wait_recv()

        @pl.when(jnp.logical_not(up_edge))
        def _():
            halo_down(s).wait_recv()

        def one(block, inner):
            attend(s, block)
            return inner

        lax.fori_loop(0, tokens // q_rows, one, 0)
        for d in range(1, n_tp):
            swap(d, s).start()
        arr[s, tp] = att[s, pl.ds(pl.multiple_of(tp * rows, rows), rows), :]
        return carry

    lax.fori_loop(0, samples, attend_step, 0)
    for i in range(pieces):
        for d in range(1, nx):
            x_send(d, i, 1).wait_recv()
            relay(d, i, 1).start()
    for i in range(pieces):
        mate_send(i, 1).wait_recv()
        for d in range(1, nx):
            relay(d, i, 1).wait_recv()

    for s in range(samples):
        for d in range(1, n_tp):
            swap(d, s).wait_recv()
        cols = slice(s * width, (s + 1) * width)
        lhs = jnp.concatenate([arr[s, t] for t in range(n_tp)], axis=1)
        mixed = jnp.dot(lhs, wo[...].reshape(-1, width), preferred_element_type=F32)
        gate = modv[s, :, 2 * width :]
        out[:, cols] = (gath[tp, s].astype(F32) + gate * mixed).astype(BF16)

    for s in range(samples):
        for d in range(1, n_tp):
            swap(d, s).wait_send()
        mate_send(s).wait_send()
        for d in range(1, nx):
            x_send(d, s).wait_send()
            relay(d, s).wait_send()

        @pl.when(jnp.logical_not(up_edge))
        def _():
            halo_up(s).wait_send()

        @pl.when(jnp.logical_not(down_edge))
        def _():
            halo_down(s).wait_send()

    for i in range(pieces):
        mate_send(i, 1).wait_send()
        for d in range(1, nx):
            x_send(d, i, 1).wait_send()
            relay(d, i, 1).wait_send()


def rope_tables(lines):
    quarter = HEAD_DIM // 4
    inverse = THETA ** (-np.arange(quarter) / quarter)
    tables = []
    for count in (lines, GRID_W):
        angles = np.tile(np.arange(count)[:, None] * inverse, (1, 8))
        sign = np.where(np.arange(128) % HEAD_DIM < HEAD_DIM // 2, -1.0, 1.0)
        tables.append(jnp.asarray(np.cos(angles), F32))
        tables.append(jnp.asarray(np.sin(angles) * sign, F32))
    return tables


def on_device(
    latents,
    context,
    condition,
    cond_context,
    w_shift,
    w_scale,
    w_gate,
    norm_gain,
    w_query,
    w_key,
    w_value,
    sink_logit,
    w_out,
):
    rows, samples, width = latents.shape
    n_tp = lax.axis_size("tp")
    n_sp = lax.axis_size("sp")
    nx = n_tp // 2
    tokens = rows * n_tp
    q_cols = w_query.shape[1]
    kv_cols = w_key.shape[1]
    ctx_rows = context.shape[0]
    mod_rows, mw = w_shift.shape
    pieces = 2
    flat = latents.reshape(rows, samples * width)
    flat_ctx = context.reshape(ctx_rows, samples * width)
    if kv_cols % 128:
        projections = (w_query, jnp.concatenate([w_key, w_value], axis=1))
    else:
        projections = (w_query, w_key, w_value)
    tables = rope_tables(n_sp * tokens // GRID_W)
    dma = pltpu.SemaphoreType.DMA
    n_move = samples + pieces
    out = pl.pallas_call(
        functools.partial(
            block_kernel, n_tp, n_sp, samples, q_cols, kv_cols, len(projections)
        ),
        out_shape=jax.ShapeDtypeStruct((rows, samples * width), BF16),
        in_specs=[VMEM] * 7
        + [pl.BlockSpec(memory_space=pltpu.SMEM)]
        + [ANY] * (6 + len(projections)),
        out_specs=VMEM,
        scratch_shapes=[
            pltpu.VMEM((n_tp, samples, rows, width), BF16),
            pltpu.VMEM((samples, ctx_rows, width), BF16),
            pltpu.VMEM((3, mod_rows, mw), BF16),
            pltpu.VMEM((width, q_cols + 2 * kv_cols), BF16),
            pltpu.VMEM((n_tp, pieces, q_cols // pieces, width), BF16),
            pltpu.VMEM((samples + 1, 1, 3 * mw), F32),
            pltpu.VMEM((n_sp, samples + 1, 1, 3 * mw), F32),
            pltpu.VMEM((n_tp, samples + 1, 1, 3 * mw), F32),
            pltpu.VMEM((samples + 1, 1, 3 * width), F32),
            pltpu.VMEM((tokens, 128), F32),
            pltpu.VMEM((tokens, 128), F32),
            pltpu.VMEM((samples, tokens, q_cols), BF16),
            pltpu.VMEM((samples, tokens + 2 * WINDOW, 2 * kv_cols), BF16),
            pltpu.VMEM((n_sp, samples, ctx_rows, 2 * kv_cols), BF16),
            pltpu.VMEM((samples, tokens, q_cols), BF16),
            pltpu.VMEM((samples, n_tp, rows, q_cols), BF16),
            dma((2 * samples + 6 + pieces,)),
            dma((n_sp,)),
            dma((n_sp,)),
            dma((n_tp,)),
            dma((n_tp,)),
            dma((nx, n_move)),
            dma((nx, n_move)),
            dma((n_move,)),
            dma((n_move,)),
            dma((nx, n_move)),
            dma((nx, n_move)),
            dma((n_sp,)),
            dma((n_sp,)),
            dma((2, samples)),
            dma((2, samples)),
            dma((n_tp, samples)),
            dma((n_tp, samples)),
        ],
        compiler_params=pltpu.CompilerParams(
            collective_id=0, has_side_effects=True, vmem_limit_bytes=VMEM_LIMIT
        ),
        name="block",
    )(
        condition,
        cond_context.reshape(1, -1),
        norm_gain.reshape(1, width),
        *tables,
        sink_logit,
        flat,
        flat_ctx,
        w_shift,
        w_scale,
        w_gate,
        w_out,
        *projections,
    )
    return out.reshape(rows, samples, width)


def solution(mesh):
    return jax.shard_map(
        on_device,
        mesh=mesh,
        in_specs=(
            P(("sp", "tp"), "grp", None),
            P("sp", "grp", None),
            P("grp", "sp"),
            P("sp"),
            P("sp", "tp"),
            P("sp", "tp"),
            P("sp", "tp"),
            P(),
            P(None, "tp"),
            P(None, "tp"),
            P(None, "tp"),
            P("tp"),
            P("tp", None),
        ),
        out_specs=P(("sp", "tp"), "grp", None),
        check_vma=False,
    )
```

time: 239 us -> 72.1 us (0.30); the launches traced: 236 us -> 71.9 us
  waiting for transfers between devices: 89.3 us -> 0 us
  Pallas kernels: 0 us -> 64.3 us
  matrix products: 37.3 us -> 0 us
  blocking collectives: 32.3 us -> 0 us
  other arithmetic: 27.7 us -> 0 us
  local copies, waits for them, and re-layouts: 30.5 us -> 7.57 us
  between operations: 13.4 us -> 0.01 us
  starting transfers between devices: 5.55 us -> 0 us
    pallas_call x0 -> x1, Pallas kernels: none -> 64.3 us  [on_device(): pl.pallas_call(functools.partial(block_kernel, n_tp, n_sp, samples, q_col...]
    all_gather x2 -> x0, waiting for transfers between devices: 51.3 us -> none  [the longest x1 31.5 us: on_device(): shard_rows = lax.all_gather(normed, 'tp', axis=0, tiled=True)]
    reduce_scatter x1 -> x0, waiting for transfers between devices: 37.9 us -> none  [on_device(): lax.psum_scatter(jnp.dot(attended, w_out, preferred_element_type=jnp.floa...]
    dot_general x10 -> x0, matrix products: 37.3 us -> none  [the longest x1 8.13 us: attend_block(): jnp.einsum('qsngd,ksnd->sngqk', q_blk, ctx_keys, preferred_element_type=j...]
    all_gather x3 -> x0, blocking collectives: 20.2 us -> none  [the longest x1 9.18 us: on_device(): lax.all_gather(sum_shift, 'tp', axis=1, tiled=True)]
    reduce_sum x4 -> x0, other arithmetic: 16.2 us -> none  [the longest x1 9.31 us: attend_block(): jnp.sum(ctx_exp, axis=-1)]
    psum x1 -> x0, blocking collectives: 12.1 us -> none  [on_device(): lax.psum((part_shift, part_scale, part_gate), 'sp')]
    convert_element_type x4 -> x0, other arithmetic: 9.13 us -> none  [the longest x2 6.11 us: modulate(): (normed * gain * (1.0 + scale_rows) + shift_rows).astype(jnp.bfloat16)]
  transfers between devices with their start and end apart: 5 -> 0, of which waited for: 3 -> 0; matrix products, arithmetic and copies ran while one was open for 9% -> 0% of each run, Pallas kernels for 0% -> 0%
where the time goes in v2:
time: 72.1 us; the launch traced here: 71.9 us
  Pallas kernels  64.3 us (89%)
  local copies, waits for them, and re-layouts  7.57 us (10%)
    pallas_call x1, Pallas kernels, on_device(): pl.pallas_call(functools.partial(block_kernel, n_tp, n_sp, samples, q_col...  64.3 us
    unnamed x4, local copies, waits for them, and re-layouts  4.95 us
    reshape x1, local copies, waits for them, and re-layouts, on_device(): return out.reshape(rows, samples, width)  2.62 us

profile of v2, /device:TPU:13, one launch (start us, length us, event | category | flops | bytes accessed | tf_op | source)
XLA Modules:
  0.0 71.9 jit_solution(12158389687852443286)
XLA Ops:
  0.0 0.0 copy-start
  0.0 2.7 %copy.18 = bf16[16,8,2,2048]{3,1,2,0:T(8,128)(2,1)} copy(bf16[16,8,2,2048]{3,2,1,0:T(2,128)(2,1)} %bitcast.9) | data formatting | bytes 2097152
  2.7 0.0 copy-done
  2.7 2.2 %copy.19 = bf16[32,8,2,2048]{3,1,2,0:T(8,128)(2,1)} copy(bf16[32,8,2,2048]{3,2,1,0:T(2,128)(2,1)S(1)} %bitcast.8) | data formatting | bytes 4194304
  5.0 64.3 %block.1 = bf16[128,4096]{1,0:T(8,128)(2,1)} custom-call(f32[2,512]{1,0:T(2,128)} %refs_0_.1, f32[1,512]{1,0:T(1,128)} %bitcast.11, f32[1,2048]{1,0:T(1,128)} %bitcast.10, f32[32,128]{1,0:T(8,128)} %constant.8.clone.refs_3_, f32[32,128]{1,0:T(8,128)} %constant.9.clone.refs_4_, f32[64,128]{1,0:T(8,128)} %constant.10.clone.refs_5_, ...), custom_call_target="tpu_custom_call" | custom-call | tf_op jit(solution)/shard_map/block/pallas_call | solution.py:494
  69.3 2.6 %reshape.19 = bf16[128,2,2048]{2,1,0:T(2,128)(2,1)} reshape(bf16[128,4096]{1,0:T(8,128)(2,1)} %block.1) | data formatting | bytes 2097152 | tf_op jit(solution)/shard_map/reshape | solution.py:556
Async XLA Ops:
  0.0 2.7 %copy-start = (bf16[256,2,2048]{2,1,0:T(2,128)(2,1)S(1)}, bf16[256,2,2048]{2,1,0:T(2,128)(2,1)}, u32[]{:S(2)}) copy-start(bf16[256,2,2048]{2,1,0:T(2,128)(2,1)} %param.18) | copy-start | bytes 6291460

commit v3 on v2

--- a/solution.py
+++ b/solution.py
@@ -80,6 +80,8 @@
         hr,
         avs,
         avr,
+        ys,
+        yr,
     ) = refs[15 + n_proj :]
     nx = n_tp // 2
     rows, width = gath.shape[2], gath.shape[3]
@@ -88,8 +90,10 @@
     per_group = q_cols // kv_cols
     sp = lax.axis_index("sp")
     tp = lax.axis_index("tp")
+    grp = lax.axis_index("grp")
     mx, core = tp // 2, lax.rem(tp, 2)
     mate = {"tp": mx * 2 + 1 - core}
+    n_grp = wo.shape[1] // samples
     pieces = wo.shape[1]
     wo_rows = wo.shape[2]
 
@@ -120,6 +124,7 @@
     enter(
         [{"tp": lax.rem(tp + d, n_tp)} for d in range(1, n_tp)]
         + [{"sp": lax.rem(sp + d, n_sp)} for d in range(1, n_sp)]
+        + [{"grp": lax.rem(grp + d, n_grp)} for d in range(1, n_grp)]
     )
 
     def spot(owner, i, kind):
@@ -140,6 +145,14 @@
         at = i + kind * samples
         piece = spot(lax.rem(mx - d + nx, nx) * 2 + core, i, kind)
         return remote(piece, piece, rs.at[d, at], rr.at[d, at], mate)
+
+    def share(e, k):
+        return lax.rem(grp - e + n_grp, n_grp) * samples + k
+
+    def y_send(d, e, k):
+        piece = spot(lax.rem(mx - d + nx, nx) * 2 + core, share(0, k), 1)
+        peer = {"grp": lax.rem(grp + e, n_grp)}
+        return remote(piece, piece, ys.at[d, e, k], yr.at[d, e, k], peer)
 
     for c in loads:
         c.wait()
@@ -195,9 +208,10 @@
             x_send(d, s).start()
     for c in outs:
         c.wait()
+    for k in range(samples):
+        for d in range(1, nx):
+            x_send(d, share(0, k), 1).start()
     for i in range(pieces):
-        for d in range(1, nx):
-            x_send(d, i, 1).start()
         mate_send(i, 1).start()
     for c in tp_sends:
         c.wait()
@@ -394,6 +408,14 @@
             halo_down(s).wait_recv()
 
         def one(block, inner):
+            @pl.when(block == tokens // q_rows // 2)
+            def _():
+                for d in range(1, nx):
+                    x_send(d, share(0, s), 1).wait_recv()
+                    for e in range(1, n_grp):
+                        y_send(d, e, s).start()
+                    relay(d, share(0, s), 1).start()
+
             attend(s, block)
             return inner
 
@@ -404,10 +426,11 @@
         return carry
 
     lax.fori_loop(0, samples, attend_step, 0)
-    for i in range(pieces):
-        for d in range(1, nx):
-            x_send(d, i, 1).wait_recv()
-            relay(d, i, 1).start()
+    for k in range(samples):
+        for d in range(1, nx):
+            for e in range(1, n_grp):
+                y_send(d, e, k).wait_recv()
+                relay(d, share(e, k), 1).start()
     for i in range(pieces):
         mate_send(i, 1).wait_recv()
         for d in range(1, nx):
@@ -438,10 +461,14 @@
         def _():
             halo_down(s).wait_send()
 
+    for k in range(samples):
+        for d in range(1, nx):
+            x_send(d, share(0, k), 1).wait_send()
+            for e in range(1, n_grp):
+                y_send(d, e, k).wait_send()
     for i in range(pieces):
         mate_send(i, 1).wait_send()
         for d in range(1, nx):
-            x_send(d, i, 1).wait_send()
             relay(d, i, 1).wait_send()
 
 
@@ -481,7 +508,7 @@
     kv_cols = w_key.shape[1]
     ctx_rows = context.shape[0]
     mod_rows, mw = w_shift.shape
-    pieces = 2
+    pieces = lax.axis_size("grp") * samples
     flat = latents.reshape(rows, samples * width)
     flat_ctx = context.reshape(ctx_rows, samples * width)
     if kv_cols % 128:
@@ -534,6 +561,8 @@
             dma((2, samples)),
             dma((n_tp, samples)),
             dma((n_tp, samples)),
+            dma((nx, pieces // samples, samples)),
+            dma((nx, pieces // samples, samples)),
         ],
         compiler_params=pltpu.CompilerParams(
             collective_id=0, has_side_effects=True, vmem_limit_bytes=VMEM_LIMIT

time: 72.1 us -> 75.3 us (1.044); the launches traced: 71.9 us -> 74.1 us
  Pallas kernels: 64.3 us -> 66.5 us
    pallas_call x1, Pallas kernels: 64.3 us -> 66.5 us  [on_device(): pl.pallas_call(functools.partial(block_kernel, n_tp, n_sp, samples, q_col...]
where the time goes in v3:
time: 75.3 us; the launch traced here: 74.1 us
  Pallas kernels  66.5 us (88%)
  local copies, waits for them, and re-layouts  7.57 us (10%)
    pallas_call x1, Pallas kernels, on_device(): pl.pallas_call(functools.partial(block_kernel, n_tp, n_sp, samples, q_col...  66.5 us
    unnamed x4, local copies, waits for them, and re-layouts  4.95 us
    reshape x1, local copies, waits for them, and re-layouts, on_device(): return out.reshape(rows, samples, width)  2.62 us

profile of v3, /device:TPU:13, one launch (start us, length us, event | category | flops | bytes accessed | tf_op | source)
XLA Modules:
  0.0 74.1 jit_solution(11614135548845419498)
XLA Ops:
  0.0 0.0 copy-start
  0.0 2.7 %copy.18 = bf16[16,8,2,2048]{3,1,2,0:T(8,128)(2,1)} copy(bf16[16,8,2,2048]{3,2,1,0:T(2,128)(2,1)} %bitcast.9) | data formatting | bytes 2097152
  2.7 0.0 copy-done
  2.7 2.2 %copy.19 = bf16[32,8,2,2048]{3,1,2,0:T(8,128)(2,1)} copy(bf16[32,8,2,2048]{3,2,1,0:T(2,128)(2,1)S(1)} %bitcast.8) | data formatting | bytes 4194304
  5.0 66.5 %block.1 = bf16[128,4096]{1,0:T(8,128)(2,1)} custom-call(f32[2,512]{1,0:T(2,128)} %refs_0_.1, f32[1,512]{1,0:T(1,128)} %bitcast.11, f32[1,2048]{1,0:T(1,128)} %bitcast.10, f32[32,128]{1,0:T(8,128)} %constant.8.clone.refs_3_, f32[32,128]{1,0:T(8,128)} %constant.9.clone.refs_4_, f32[64,128]{1,0:T(8,128)} %constant.10.clone.refs_5_, ...), custom_call_target="tpu_custom_call" | custom-call | tf_op jit(solution)/shard_map/block/pallas_call | solution.py:521
  71.5 2.6 %reshape.19 = bf16[128,2,2048]{2,1,0:T(2,128)(2,1)} reshape(bf16[128,4096]{1,0:T(8,128)(2,1)} %block.1) | data formatting | bytes 2097152 | tf_op jit(solution)/shard_map/reshape | solution.py:585
Async XLA Ops:
  0.0 2.7 %copy-start = (bf16[256,2,2048]{2,1,0:T(2,128)(2,1)S(1)}, bf16[256,2,2048]{2,1,0:T(2,128)(2,1)}, u32[]{:S(2)}) copy-start(bf16[256,2,2048]{2,1,0:T(2,128)(2,1)} %param.18) | copy-start | bytes 6291460
